TPU v7x, 128 devices: a whole 4x4x4 slice. The times are simulated.
128 devices in a mesh: sp: 16 (over z, x), tp: 8 (over y, core).
Axes of the slice: x: 4, y: 4, z: 4, core: 2. Of those that a mesh axis runs over, the one named last changes fastest.
Arguments:
- queries: bfloat16 [8192, 2048], P('sp', 'tp'), may hold values from -6 to 6
- keys: bfloat16 [8192, 1024], P('sp', 'tp'), may hold values from -6 to 6
- values: bfloat16 [8192, 1024], P('sp', 'tp'), may hold values from -6 to 6
- documents: int32 [8192], P('sp'), may hold values from 0 to 3, never falling along the last dimension, each value on 1 to 4096 neighbouring positions
- query_gain: float32 [128], replicated, may hold values from 1.8 to 6
- key_gain: float32 [128], replicated, may hold values from 1.8 to 6
- residual: bfloat16 [8192, 4096], P('sp', 'tp'), may hold values from -6 to 6
- out_weight: bfloat16 [2048, 4096], P('tp'), may hold values from -0.125 to 0.125
- norm_gain: float32 [4096], replicated, may hold values from 0.1 to 1.9
- up_weight: bfloat16 [4096, 16384], P('sp', 'tp'), may hold values from -0.09375 to 0.09375
- down_weight: bfloat16 [16384, 4096], P('tp', 'sp'), may hold values from -0.046875 to 0.046875
Outputs:
- mixed: bfloat16 [8192, 4096], P('sp', 'tp')
Inputs may be any that keep to these rules, and one draw needn't show every extreme that they name: `documents`: document numbers never fall along the sequence; a document has at most 4096 positions.
All inputs are finite; a program needn't handle non-finite values.
Results may differ from a plain program's by a relative error of at most 0.017.
The roundings to bfloat16 on the way count: a program that leaves them out, or rounds other values in their place, can miss the bound.
Values may be sent and summed in bfloat16 or wider, within the bound.
A program may use at most 192 MiB of HBM per device.

v0:
```python
import jax
import jax.numpy as jnp
from jax import lax
from jax.sharding import Mesh
from jax.sharding import PartitionSpec as P

D = 4096
HQ = 16
KV = 8
HD = 128
GRID_W = 64
TP = ("tp_0", "tp_1")
norm_eps = 1e-06
rope_base = 10000.0
masked_score = -1e30


def gather_turned(arrays, axis, dims):
    turned = [jnp.moveaxis(a, dim, 0) for a, dim in zip(arrays, dims)]
    both = jnp.concatenate([t.reshape(len(t), -1) for t in turned], axis=1)
    filled, at, finished = (lax.all_gather(both, axis, axis=0, tiled=True), 0, [])
    for t, dim in zip(turned, dims):
        section = filled[:, at : at + t[0].size].reshape(-1, *t.shape[1:])
        finished.append(jnp.moveaxis(section, 0, dim))
        at += t[0].size
    return tuple(finished)


def in_one_piece(arrays, axis, dim, along):
    columns = [a.reshape(*a.shape[:along], -1) for a in arrays]
    both = jnp.concatenate(columns, axis=along)
    filled, at, finished = (lax.all_gather(both, axis, axis=dim, tiled=True), 0, [])
    for a, column in zip(arrays, columns):
        section = filled[..., at : at + column.shape[along]]
        finished.append(section.reshape(*section.shape[:along], *a.shape[along:]))
        at += column.shape[along]
    return tuple(finished)


def split_up(x, dim, size):
    dims = x.shape
    pieces = x.reshape(*dims[:dim], size, dims[dim] // size, *dims[dim + 1 :])
    return jnp.moveaxis(pieces, dim, 0)


def sum_at_owner(x, axis, dim):
    pieces = split_up(x, dim, lax.axis_size(axis))
    arrived = lax.all_to_all(pieces, axis, split_axis=0, concat_axis=0, tiled=True)
    return arrived.astype(jnp.float32).sum(axis=0)


def sent_to_all(x, axis):
    copies = jnp.broadcast_to(x, (lax.axis_size(axis), *x.shape))
    return lax.all_to_all(copies, axis, split_axis=0, concat_axis=0, tiled=True)


def over_copies(x, axis):
    return sent_to_all(x, axis).sum(axis=0)


def joined_along(pieces, dim):
    pieces = jnp.moveaxis(pieces, 0, dim)
    dims = pieces.shape
    return pieces.reshape(*dims[:dim], dims[dim] * dims[dim + 1], *dims[dim + 2 :])


def whole_of(x, axes, dim):
    far, near = axes
    initial = sent_to_all(x, far)
    pieces = jnp.swapaxes(sent_to_all(initial, near), 0, 1)
    return joined_along(pieces.reshape(-1, *x.shape), dim)


def head_norm(heads_in, gain):
    values32 = heads_in.astype(jnp.float32)
    scaled = values32 * lax.rsqrt(jnp.mean(values32 * values32, axis=-1, keepdims=True) + norm_eps)
    return scaled * gain


def rotate_half(heads_in, position):
    quarter = heads_in.shape[-1] // 2
    inverse_freq = rope_base ** (-jnp.arange(quarter, dtype=jnp.float32) / quarter)
    angles = position[:, None] * inverse_freq[None, :]
    cosine_part = jnp.cos(angles)[:, None, :]
    sine_part = jnp.sin(angles)[:, None, :]
    leading = heads_in[..., :quarter]
    trailing = heads_in[..., quarter:]
    return jnp.concatenate(
        [
            leading * cosine_part - trailing * sine_part,
            leading * sine_part + trailing * cosine_part,
        ],
        axis=-1,
    )


def grid_rotary(heads_in, positions):
    half_width = heads_in.shape[-1] // 2
    grid_row = (positions // GRID_W).astype(jnp.float32)
    grid_col = (positions % GRID_W).astype(jnp.float32)
    return jnp.concatenate(
        [
            rotate_half(heads_in[..., :half_width], grid_row),
            rotate_half(heads_in[..., half_width:], grid_col),
        ],
        axis=-1,
    )


def body(
    queries,
    keys,
    values,
    documents,
    query_gain,
    key_gain,
    residual,
    out_weight,
    norm_gain,
    up_weight,
    down_weight,
):
    tok_rows = queries.shape[0]
    key_heads = keys.shape[1] // HD
    group_size = HQ // KV
    width_local = residual.shape[1]
    tp_index = lax.axis_index(TP)
    up_whole, down_whole = gather_turned((up_weight, down_weight), "sp", (0, 1))
    positions = lax.axis_index("sp") * tok_rows + jnp.arange(tok_rows, dtype=jnp.int32)
    queries_rot = grid_rotary(
        head_norm(queries.reshape(tok_rows, key_heads * group_size, HD), query_gain), positions
    )
    queries_rot = queries_rot.astype(jnp.bfloat16).reshape(tok_rows, key_heads, group_size, HD)
    keys_rot = grid_rotary(
        head_norm(keys.reshape(tok_rows, key_heads, HD), key_gain), positions
    ).astype(jnp.bfloat16)
    value_heads = values.reshape(tok_rows, key_heads, HD)
    own_docs = documents.astype(jnp.bfloat16)
    score_scale = HD ** (-0.5)
    running_max = jnp.full((key_heads, group_size, tok_rows), masked_score, jnp.float32)
    key_piece, value_piece, doc_piece = in_one_piece((keys_rot, value_heads, own_docs), "sp", 0, 1)
    scores = (
        jnp.einsum("qkgd,skd->kgqs", queries_rot, key_piece, preferred_element_type=jnp.float32)
        * score_scale
    )
    same_doc = own_docs[:, None] == doc_piece[None, :]
    scores = jnp.where(same_doc, scores, masked_score)
    new_max = jnp.maximum(running_max, jnp.max(scores, axis=-1))
    probs = jnp.where(same_doc, jnp.exp(scores - new_max[..., None]), 0.0)
    running_sum = jnp.sum(probs, axis=-1)
    update = jnp.einsum(
        "kgqs,skd->qkgd",
        probs.astype(jnp.bfloat16),
        value_piece,
        preferred_element_type=jnp.float32,
    )
    weighted = update
    running_max, running_sum, weighted = (new_max, running_sum, weighted)
    attended = (weighted / jnp.transpose(running_sum, (2, 0, 1))[..., None]).astype(jnp.bfloat16)
    attended = attended.reshape(tok_rows, key_heads * group_size * HD)
    partial_out = jnp.dot(attended, out_weight, preferred_element_type=jnp.float32)
    branch = sum_at_owner(partial_out.astype(jnp.bfloat16), TP, 1)
    stream = residual.astype(jnp.float32) + branch
    square_sum = over_copies(jnp.sum(stream * stream, axis=-1), TP)
    gain_local = lax.dynamic_slice_in_dim(norm_gain, tp_index * width_local, width_local, 0)
    normed_local = stream * lax.rsqrt(square_sum[:, None] / D + norm_eps) * gain_local
    normed = whole_of(normed_local.astype(jnp.bfloat16), ("tp_0", "tp_1"), 1)
    hidden = jnp.dot(normed, up_whole, preferred_element_type=jnp.float32)
    positive = jnp.maximum(hidden, 0.0)
    squared = (positive * positive).astype(jnp.bfloat16)
    product = jnp.dot(squared, down_whole, preferred_element_type=jnp.float32)
    feed = lax.psum_scatter(
        product.astype(jnp.bfloat16), TP, scatter_dimension=1, tiled=True
    ).astype(jnp.float32)
    return (stream + feed).astype(jnp.bfloat16)


def solution(mesh):
    split = Mesh(mesh.devices.reshape(mesh.shape["sp"], 4, 2), ("sp", "tp_0", "tp_1"))
    return jax.shard_map(
        body,
        mesh=split,
        in_specs=(
            P("sp", TP),
            P("sp", TP),
            P("sp", TP),
            P("sp"),
            P(),
            P(),
            P("sp", TP),
            P(TP, None),
            P(),
            P("sp", TP),
            P(TP, "sp"),
        ),
        out_specs=P("sp", TP),
        check_vma=False,
    )
```

profile of v0, /device:TPU:0, one launch (start us, length us, event | category | flops | bytes accessed | tf_op | source)
XLA Modules:
  0.0 357.3 jit_solution(17306286537889101392)
XLA Ops:
  6.6 1.2 copy.50
  10.5 1.8 concatenate.30
  12.4 1.5 copy.64
  13.9 2.7 pad_maximum_fusion
  17.0 1.9 multiply_cosine_fusion.1
  19.6 56.8 %all-gather.3.cloned.1.call-done = bf16[8192,257]{1,0:T(8,128)(2,1)} async-done(((bf16[512,257]{1,0:T(8,128)(2,1)}), bf16[8192,257]{1,0:T(8,128)(2,1)}) %all-gather.3.cloned.1.call-update) | async-done | bytes 4210704 | tf_op jit(solution)/shard_map/all_gather | solution.py:32
  76.4 2.2 slice_reduce_fusion
  78.7 4.0 %broadcast_compare_fusion = pred[512,8192]{0,1:T(8,128)(4,1)} fusion(bf16[512]{0:T(512)(128)(2,1)S(1)} %convert_element_type.70, bf16[8192]{0:T(1024)(128)(2,1)S(1)} %slice_reduce_fusion), kind=kLoop, calls=%fused_computation.17 | loop fusion | flops 4194304 | bytes 4211712 | tf_op jit(solution)/shard_map/eq | solution.py:146
  82.6 17.1 %fusion = (f32[2,512]{1,0:T(2,128)S(1)}, f32[8192,512,2]{1,0,2:T(8,128)}) fusion(pred[512,8192]{0,1:T(8,128)(4,1)} %broadcast_compare_fusion, bf16[512,2,32]{2,0,1:T(8,128)(2,1)S(1)} %get-tuple-element.9, bf16[512,2,32]{2,0,1:T(8,128)(2,1)S(1)} %get-tuple-element.10, bf16[512,2,32]{2,0,1:T(8,128)(2,1)S(1)} %get-tuple-element.6, ...), kind=kOutput, calls=%fused_computation.2 | convolution fusion | flops 2173697024 | bytes 40112128 | tf_op jit(solution)/shard_map/qkgd,skd->kgqs/dot_general | solution.py:143
  99.7 15.8 %fusion.1 = f32[2,512]{1,0:T(2,128)S(1)} fusion(f32[8192,512,2]{1,0,2:T(8,128)} %get-tuple-element.24, f32[2,512]{1,0:T(2,128)S(1)} %broadcast_maximum_fusion, pred[512,8192]{0,1:T(8,128)(4,1)} %broadcast_compare_fusion), kind=kLoop, calls=%fused_computation.3 | loop fusion | flops 41942016 | bytes 37756928 | tf_op jit(solution)/shard_map/reduce_sum | solution.py:150
  115.6 17.6 %fusion.26 = bf16[512,1,2,128]{0,3,2,1:T(8,128)(2,1)S(1)} fusion(f32[8192,512,2]{1,0,2:T(8,128)} %get-tuple-element.24, f32[2,512]{1,0:T(2,128)S(1)} %broadcast_maximum_fusion, pred[512,8192]{0,1:T(8,128)(4,1)} %broadcast_compare_fusion, bf16[8192,257]{1,0:T(8,128)(2,1)} %all-gather.3.cloned.1.call-done, f32[512,2]{0,1:T(2,128)S(1)} %bitcast.100), kind=kOutput, calls=%fused_computation.30 | convolution fusion | flops 2189688832 | bytes 40116224 | tf_op jit(solution)/shard_map/kgqs,skd->qkgd/dot_general | solution.py:151
  133.1 1.3 convolution_convert_fusion
  134.8 53.9 %all_to_all.21 = bf16[8,512,512]{2,1,0:T(8,128)(2,1)S(1)} all-to-all(bf16[8,512,512]{2,1,0:T(8,128)(2,1)S(1)} %bitcast.94), channel_id=1, replica_groups=mesh['sp'=16,'tp_0'=4,'tp_1'=2] {'tp_0','tp_1'}, dimensions={0} | all-to-all | bytes 8388608 | tf_op jit(solution)/shard_map/all_to_all | solution.py:48
  190.2 3.3 all-to-all-start.1
  194.4 4.5 %all-to-all-done.1 = f32[8,1,512]{2,1,0:T(1,128)S(1)} async-done(((f32[8,1,512]{2,1,0:T(1,128)}), f32[8,1,512]{2,1,0:T(1,128)S(1)}, u32[]{:S(2)}, u32[]{:S(2)}) %all-to-all-start.1) | async-done | bytes 16416 | tf_op jit(solution)/shard_map/all_to_all | solution.py:54
  199.2 29.1 %all_to_all.22 = bf16[4,512,512]{2,1,0:T(8,128)(2,1)S(1)} all-to-all(bf16[4,512,512]{2,1,0:T(8,128)(2,1)S(1)} %broadcast_in_dim.23), channel_id=1, replica_groups=mesh['sp'=16,'tp_0'=4,'tp_1'=2] {'tp_0'}, dimensions={0} | all-to-all | bytes 4194304 | tf_op jit(solution)/shard_map/all_to_all | solution.py:54
  228.7 7.1 %all_to_all.23 = bf16[2,4,512,512]{3,2,1,0:T(8,128)(2,1)S(1)} all-to-all(bf16[2,4,512,512]{3,2,1,0:T(8,128)(2,1)S(1)} %broadcast_in_dim.26), channel_id=1, replica_groups=mesh['sp'=16,'tp_0'=4,'tp_1'=2] {'tp_1'}, dimensions={0} | all-to-all | bytes 8388608 | tf_op jit(solution)/shard_map/all_to_all | solution.py:54
  235.8 2.4 copy.62
  238.2 6.5 %copy.63 = bf16[512,8,512]{0,2,1:T(8,128)(2,1)} copy(bf16[512,8,512]{2,0,1:T(8,128)(2,1)} %bitcast.95) | data formatting | bytes 8388608 | tf_op jit(solution)/shard_map/transpose | solution.py:62
  244.8 38.8 %all-gather.5.cloned.1.call-done = bf16[4096,4096]{0,1:T(8,128)(2,1)} async-done(((bf16[256,4096]{0,1:T(8,128)(2,1)}), bf16[4096,4096]{0,1:T(8,128)(2,1)}) %all-gather.5.cloned.1.call-update) | async-done | bytes 33554448 | tf_op jit(solution)/shard_map/all_gather | solution.py:21
  283.6 13.7 %multiply_convert_fusion.clone.5 = bf16[512,2048]{1,0:T(8,128)(2,1)S(1)} fusion(bf16[512,4096]{0,1:T(8,128)(2,1)} %bitcast.96, bf16[4096,4096]{0,1:T(8,128)(2,1)} %all-gather.5.cloned.1.call-done), kind=kOutput, calls=%fused_computation.16.clone.clone.clone.2 | convolution fusion | flops 8593080320 | bytes 23068672 | tf_op jit(solution)/shard_map/dot_general | solution.py:168
  297.3 13.9 %fusion.11 = bf16[512,4096]{1,0:T(8,128)(2,1)} fusion(bf16[4096,4096]{0,1:T(8,128)(2,1)} %all-gather.5.cloned.1.call-done, bf16[512,2048]{1,0:T(8,128)(2,1)S(1)} %multiply_convert_fusion.clone.5), kind=kOutput, calls=%fused_computation.13 | convolution fusion | flops 8592031744 | bytes 23068672 | tf_op jit(solution)/shard_map/dot_general | solution.py:171
  311.3 37.3 %reduce-scatter.2.cloned.1.call-done = bf16[512,512]{1,0:T(8,128)(2,1)} async-done(((bf16[512,4096]{1,0:T(8,128)(2,1)}), bf16[512,512]{1,0:T(8,128)(2,1)}) %reduce-scatter.2.cloned.1.call-update) | async-done | bytes 524304 | tf_op jit(solution)/shard_map/reduce_scatter | solution.py:172
  348.6 2.2 add_convert_fusion
  (45 shorter events, 7.2 us)
Async XLA Ops:
  6.5 126.6 %copy-start = (bf16[256,4096]{1,0:T(8,128)(2,1)S(1)}, bf16[256,4096]{1,0:T(8,128)(2,1)}, u32[]{:S(2)}) copy-start(bf16[256,4096]{1,0:T(8,128)(2,1)} %param.18) | copy-start | bytes 6291460
  6.5 10.1 %copy-start.3 = (bf16[512,256]{1,0:T(8,128)(2,1)S(1)}, bf16[512,256]{1,0:T(8,128)(2,1)}, u32[]{:S(2)}) copy-start(bf16[512,256]{1,0:T(8,128)(2,1)} %param.11) | copy-start | bytes 786436
  6.5 69.9 %all-gather.3.cloned.1.call-start = ((), (), s32[]{:S(2)}) async-start(), calls=%async_computation.5 | async-start | bytes 6684672 | tf_op jit(solution)/shard_map/all_gather | solution.py:32
  10.5 8.4 %copy-start.4 = (f32[128]{0:T(128)S(1)}, f32[128]{0:T(128)}, u32[]{:S(2)}) copy-start(f32[128]{0:T(128)} %param.15) | copy-start | bytes 1540
  12.4 271.2 %all-gather.5.cloned.1.call-start = ((), (), s32[]{:S(2)}) async-start(), calls=%async_computation.6 | async-start | bytes 35651584 | tf_op jit(solution)/shard_map/all_gather | solution.py:21
  134.8 54.5 %copy-start.2 = (bf16[512,512]{1,0:T(8,128)(2,1)S(1)}, bf16[512,512]{1,0:T(8,128)(2,1)}, u32[]{:S(2)}) copy-start(bf16[512,512]{1,0:T(8,128)(2,1)} %param.17) | copy-start | bytes 1572868
  190.2 8.6 %all-to-all-start.1 = ((f32[8,1,512]{2,1,0:T(1,128)}), f32[8,1,512]{2,1,0:T(1,128)S(1)}, u32[]{:S(2)}, u32[]{:S(2)}) async-start(f32[8,1,512]{2,1,0:T(1,128)} %broadcast_in_dim.22), calls=%async_computation.1 | async-start | bytes 32768 | tf_op jit(solution)/shard_map/all_to_all | solution.py:54
  193.6 155.0 %reduce-scatter.2.cloned.1.call-start = ((), (), s32[]{:S(2)}) async-start(), calls=%async_computation.7 | async-start | bytes 4718592 | tf_op jit(solution)/shard_map/reduce_scatter | solution.py:172
  297.3 53.5 %copy-start.1 = (bf16[256,4096]{1,0:T(8,128)(2,1)S(1)}, bf16[256,4096]{1,0:T(8,128)(2,1)}, u32[]{:S(2)}) copy-start(bf16[256,4096]{1,0:T(8,128)(2,1)} %param.18) | copy-start | bytes 6291460
Sparse Core Ops, SparseCore 0:
  12.5 63.8 all-gather.2
  78.5 204.9 all-gather.4
  311.4 37.1 reduce-scatter.1
where the time goes:
time: 358 us; the launch traced here: 357 us
  waiting for transfers between devices  137 us (38%)
  blocking collectives  90.2 us (25%)
  matrix products  63.6 us (18%)
  other arithmetic  30.5 us (9%)
  local copies, waits for them, and re-layouts  18.9 us (5%)
  between operations  13.3 us (4%)
    all_gather x1, waiting for transfers between devices, in_one_piece(): lax.all_gather(both, axis, axis=dim, tiled=True)  56.8 us
    all_to_all x1, blocking collectives, sum_at_owner(): lax.all_to_all(pieces, axis, split_axis=0, concat_axis=0, tiled=True)  53.9 us
    all_gather x1, waiting for transfers between devices, gather_turned(): lax.all_gather(both, axis, axis=0, tiled=True)  38.8 us
    reduce_scatter x1, waiting for transfers between devices, body(): lax.psum_scatter(product.astype(jnp.bfloat16), TP, scatter_dimension=1, t...  37.3 us
    all_to_all x2, blocking collectives, sent_to_all(): return lax.all_to_all(copies, axis, split_axis=0, concat_axis=0, tiled=True)  36.2 us
    dot_general x1, matrix products, body(): jnp.einsum('kgqs,skd->qkgd', probs.astype(jnp.bfloat16), value_piece, pre...  17.6 us
    dot_general x1, matrix products, body(): jnp.einsum('qkgd,skd->kgqs', queries_rot, key_piece, preferred_element_ty...  17.1 us
    reduce_sum x1, other arithmetic, body(): running_sum = jnp.sum(probs, axis=-1)  15.8 us
  transfers between devices with their start and end apart: 4, of which 4 were waited for; matrix products, arithmetic and copies ran while one was open for 22% of the time, Pallas kernels for 0%

commit v1 on v0

--- a/solution.py
+++ b/solution.py
@@ -15,10 +15,15 @@
 masked_score = -1e30
 
 
+def exchange_gather(x, axis, dim):
+    stack = jnp.stack([x] * lax.axis_size(axis))
+    return jnp.concatenate(lax.all_to_all(stack, axis, 0, 0), axis=dim)
+
+
 def gather_turned(arrays, axis, dims):
     turned = [jnp.moveaxis(a, dim, 0) for a, dim in zip(arrays, dims)]
     both = jnp.concatenate([t.reshape(len(t), -1) for t in turned], axis=1)
-    filled, at, finished = (lax.all_gather(both, axis, axis=0, tiled=True), 0, [])
+    filled, at, finished = (exchange_gather(both, axis, 0), 0, [])
     for t, dim in zip(turned, dims):
         section = filled[:, at : at + t[0].size].reshape(-1, *t.shape[1:])
         finished.append(jnp.moveaxis(section, 0, dim))

time: 358 us -> 829 us (2.32)
  waiting for transfers between devices: 137 us -> 607 us
  blocking collectives: 90.2 us -> 62.2 us
  local copies, waits for them, and re-layouts: 18.9 us -> 38.9 us
  starting transfers between devices: 3.42 us -> 12.9 us
    all_to_all x0 -> x1, waiting for transfers between devices: none -> 494 us  [exchange_gather(): return jnp.concatenate(lax.all_to_all(stack, axis, 0, 0), axis=dim)]
    all_gather x1 -> x0, waiting for transfers between devices: 38.8 us -> none  [gather_turned(): lax.all_gather(both, axis, axis=0, tiled=True)]
    all_to_all x2 -> x1, blocking collectives: 36.2 us -> 8.28 us  [sent_to_all(): return lax.all_to_all(copies, axis, split_axis=0, concat_axis=0, tiled=True)]
    all_to_all x1 -> x2, waiting for transfers between devices: 4.45 us -> 21.7 us  [sent_to_all(): return lax.all_to_all(copies, axis, split_axis=0, concat_axis=0, tiled=True)]
    another operation x0 -> x1, local copies, waits for them, and re-layouts: none -> 10.9 us  [exchange_gather(): stack = jnp.stack([x] * lax.axis_size(axis))]
  transfers between devices with their start and end apart: 4 -> 5, of which waited for: 4 -> 5; matrix products, arithmetic and copies ran while one was open for 22% -> 3% of each run, Pallas kernels for 0% -> 0%
where the time goes in v1:
time: 829 us
  waiting for transfers between devices  607 us (73%)
  blocking collectives  62.2 us (8%)
  matrix products  61.6 us (7%)
  local copies, waits for them, and re-layouts  38.9 us (5%)
  other arithmetic  32 us (4%)
  between operations  13.6 us (2%)
  starting transfers between devices  12.9 us (2%)
    all_to_all x1, waiting for transfers between devices, exchange_gather(): return jnp.concatenate(lax.all_to_all(stack, axis, 0, 0), axis=dim)  494 us
    all_gather x1, waiting for transfers between devices, in_one_piece(): lax.all_gather(both, axis, axis=dim, tiled=True)  58.8 us
    all_to_all x1, blocking collectives, sum_at_owner(): lax.all_to_all(pieces, axis, split_axis=0, concat_axis=0, tiled=True)  53.9 us
    reduce_scatter x1, waiting for transfers between devices, body(): lax.psum_scatter(product.astype(jnp.bfloat16), TP, scatter_dimension=1, t...  33.2 us
    all_to_all x2, waiting for transfers between devices, sent_to_all(): return lax.all_to_all(copies, axis, split_axis=0, concat_axis=0, tiled=True)  21.7 us
    dot_general x1, matrix products, body(): jnp.einsum('kgqs,skd->qkgd', probs.astype(jnp.bfloat16), value_piece, pre...  17 us
  transfers between devices with their start and end apart: 5, of which 5 were waited for; matrix products, arithmetic and copies ran while one was open for 3% of the time, Pallas kernels for 0%

profile of v1, /device:TPU:0, one launch (start us, length us, event | category | flops | bytes accessed | tf_op | source)
XLA Modules:
  0.0 828.5 jit_solution(275133400649175441)
XLA Ops:
  17.5 58.8 %all-gather.2.cloned.1.call-done = bf16[8192,257]{1,0:T(8,128)(2,1)} async-done(((bf16[512,257]{1,0:T(8,128)(2,1)}), bf16[8192,257]{1,0:T(8,128)(2,1)}) %all-gather.2.cloned.1.call-update) | async-done | bytes 4210704 | tf_op jit(solution)/shard_map/all_gather | solution.py:37
  76.4 2.2 slice_reduce_fusion
  78.6 4.0 broadcast_compare_fusion
  82.7 15.7 %fusion = (f32[2,512]{1,0:T(2,128)S(1)}, f32[8192,512,2]{1,0,2:T(8,128)}) fusion(pred[512,8192]{0,1:T(8,128)(4,1)} %broadcast_compare_fusion, bf16[512,2,32]{2,0,1:T(8,128)(2,1)S(1)} %get-tuple-element.9, bf16[512,2,32]{2,0,1:T(8,128)(2,1)S(1)} %copy-done.4, bf16[512,2,32]{2,0,1:T(8,128)(2,1)S(1)} %get-tuple-element.6, ...), kind=kOutput, calls=%fused_computation.2 | convolution fusion | flops 2173697024 | bytes 40112128 | tf_op jit(solution)/shard_map/qkgd,skd->kgqs/dot_general | solution.py:148
  98.4 15.6 %fusion.1 = f32[2,512]{1,0:T(2,128)S(1)} fusion(f32[8192,512,2]{1,0,2:T(8,128)} %get-tuple-element.24, f32[2,512]{1,0:T(2,128)S(1)} %broadcast_maximum_fusion, pred[512,8192]{0,1:T(8,128)(4,1)} %broadcast_compare_fusion), kind=kLoop, calls=%fused_computation.3 | loop fusion | flops 41942016 | bytes 37756928 | tf_op jit(solution)/shard_map/reduce_sum | solution.py:155
  114.0 17.0 %fusion.26 = bf16[512,1,2,128]{0,3,2,1:T(8,128)(2,1)S(1)} fusion(f32[8192,512,2]{1,0,2:T(8,128)} %get-tuple-element.24, f32[2,512]{1,0:T(2,128)S(1)} %broadcast_maximum_fusion, pred[512,8192]{0,1:T(8,128)(4,1)} %broadcast_compare_fusion, bf16[8192,257]{1,0:T(8,128)(2,1)} %all-gather.2.cloned.1.call-done, f32[512,2]{0,1:T(2,128)S(1)} %bitcast.101), kind=kOutput, calls=%fused_computation.30 | convolution fusion | flops 2189688832 | bytes 40116224 | tf_op jit(solution)/shard_map/kgqs,skd->qkgd/dot_general | solution.py:156
  132.6 53.9 %all_to_all.26 = bf16[8,512,512]{2,1,0:T(8,128)(2,1)S(1)} all-to-all(bf16[8,512,512]{2,1,0:T(8,128)(2,1)S(1)} %bitcast.95), channel_id=1, replica_groups=mesh['sp'=16,'tp_0'=4,'tp_1'=2] {'tp_0','tp_1'}, dimensions={0} | all-to-all | bytes 8388608 | tf_op jit(solution)/shard_map/all_to_all | solution.py:53
  188.0 3.3 all-to-all-start.1
  192.1 4.5 all-to-all-done.1
  198.4 3.6 all-to-all-start.2
  202.0 2.3 copy.69
  204.3 3.0 pad_maximum_fusion
  207.3 4.1 copy.70
  211.4 17.1 %all-to-all-done.2 = bf16[4,512,512]{2,1,0:T(8,128)(2,1)S(1)} async-done(((bf16[4,512,512]{2,1,0:T(8,128)(2,1)}), bf16[4,512,512]{2,1,0:T(8,128)(2,1)S(1)}, u32[]{:S(2)}, u32[]{:S(2)}) %all-to-all-start.2) | async-done | bytes 2097184 | tf_op jit(solution)/shard_map/all_to_all | solution.py:59
  228.9 8.3 all_to_all.27
  237.2 10.9 %stack.2 = bf16[16,256,4096]{2,1,0:T(8,128)(2,1)} broadcast(bf16[256,4096]{1,0:T(8,128)(2,1)S(1)} %copy-done.2), dimensions={1,2} | broadcast | bytes 35651584 | tf_op jit(solution)/shard_map/stack | solution.py:19
  248.1 6.0 all-to-all-start.4
  254.1 4.4 copy.67
  258.5 6.5 copy.68
  264.9 493.6 %all-to-all-done.4 = bf16[16,256,4096]{2,1,0:T(8,128)(2,1)} async-done(((bf16[16,256,4096]{2,1,0:T(8,128)(2,1)}), bf16[16,256,4096]{2,1,0:T(8,128)(2,1)}, u32[]{:S(2)}, u32[]{:S(2)}) %all-to-all-start.4) | async-done | bytes 33554464 | tf_op jit(solution)/shard_map/all_to_all | solution.py:20
  758.6 13.6 %multiply_convert_fusion.clone.5 = bf16[512,2048]{1,0:T(8,128)(2,1)S(1)} fusion(bf16[512,4096]{0,1:T(8,128)(2,1)} %bitcast.97, bf16[4096,4096]{1,0:T(8,128)(2,1)} %bitcast.24), kind=kOutput, calls=%fused_computation.16.clone.clone.clone.2 | convolution fusion | flops 8593080320 | bytes 23068672 | tf_op jit(solution)/shard_map/dot_general | solution.py:173
  772.2 14.0 %fusion.11 = bf16[512,4096]{1,0:T(8,128)(2,1)} fusion(bf16[4096,4096]{1,0:T(8,128)(2,1)} %bitcast.24, bf16[512,2048]{1,0:T(8,128)(2,1)S(1)} %multiply_convert_fusion.clone.5), kind=kOutput, calls=%fused_computation.13 | convolution fusion | flops 8592031744 | bytes 23068672 | tf_op jit(solution)/shard_map/dot_general | solution.py:176
  786.3 33.2 %reduce-scatter.2.cloned.1.call-done = bf16[512,512]{1,0:T(8,128)(2,1)} async-done(((bf16[512,4096]{1,0:T(8,128)(2,1)}), bf16[512,512]{1,0:T(8,128)(2,1)}) %reduce-scatter.2.cloned.1.call-update) | async-done | bytes 524304 | tf_op jit(solution)/shard_map/reduce_scatter | solution.py:177
  819.5 2.2 add_convert_fusion
  (47 shorter events, 17.0 us)
Async XLA Ops:
  6.5 124.4 %copy-start = (bf16[256,4096]{1,0:T(8,128)(2,1)S(1)}, bf16[256,4096]{1,0:T(8,128)(2,1)}, u32[]{:S(2)}) copy-start(bf16[256,4096]{1,0:T(8,128)(2,1)} %param.18) | copy-start | bytes 6291460
  6.5 69.8 %all-gather.2.cloned.1.call-start = ((), (), s32[]{:S(2)}) async-start(), calls=%async_computation.6 | async-start | bytes 6684672 | tf_op jit(solution)/shard_map/all_gather | solution.py:37
  17.5 65.1 %copy-start.4 = (bf16[512,2,32]{2,0,1:T(8,128)(2,1)S(1)}, bf16[512,2,32]{2,0,1:T(8,128)(2,1)}, u32[]{:S(2)}) copy-start(bf16[512,2,32]{2,0,1:T(8,128)(2,1)} %get-tuple-element.10) | copy-start | bytes 196612
  132.6 54.5 %copy-start.3 = (bf16[512,512]{1,0:T(8,128)(2,1)S(1)}, bf16[512,512]{1,0:T(8,128)(2,1)}, u32[]{:S(2)}) copy-start(bf16[512,512]{1,0:T(8,128)(2,1)} %param.17) | copy-start | bytes 1572868
  188.0 8.6 %all-to-all-start.1 = ((f32[8,1,512]{2,1,0:T(1,128)}), f32[8,1,512]{2,1,0:T(1,128)S(1)}, u32[]{:S(2)}, u32[]{:S(2)}) async-start(f32[8,1,512]{2,1,0:T(1,128)} %broadcast_in_dim.22), calls=%async_computation.1 | async-start | bytes 32768 | tf_op jit(solution)/shard_map/all_to_all | solution.py:59
  198.4 30.2 %all-to-all-start.2 = ((bf16[4,512,512]{2,1,0:T(8,128)(2,1)}), bf16[4,512,512]{2,1,0:T(8,128)(2,1)S(1)}, u32[]{:S(2)}, u32[]{:S(2)}) async-start(bf16[4,512,512]{2,1,0:T(8,128)(2,1)} %broadcast_in_dim.23), calls=%async_computation.2 | async-start | bytes 4194304 | tf_op jit(solution)/shard_map/all_to_all | solution.py:59
  228.5 8.7 %copy-start.2 = (bf16[256,4096]{1,0:T(8,128)(2,1)S(1)}, bf16[256,4096]{1,0:T(8,128)(2,1)}, u32[]{:S(2)}) copy-start(bf16[256,4096]{1,0:T(8,128)(2,1)} %copy.70) | copy-start | bytes 6291460
  248.1 510.5 %all-to-all-start.4 = ((bf16[16,256,4096]{2,1,0:T(8,128)(2,1)}), bf16[16,256,4096]{2,1,0:T(8,128)(2,1)}, u32[]{:S(2)}, u32[]{:S(2)}) async-start(bf16[16,256,4096]{2,1,0:T(8,128)(2,1)} %stack.2), calls=%async_computation.4 | async-start | bytes 67108864 | tf_op jit(solution)/shard_map/all_to_all | solution.py:20
  254.0 565.4 %reduce-scatter.2.cloned.1.call-start = ((), (), s32[]{:S(2)}) async-start(), calls=%async_computation.7 | async-start | bytes 4718592 | tf_op jit(solution)/shard_map/reduce_scatter | solution.py:177
  772.2 49.5 %copy-start.1 = (bf16[256,4096]{1,0:T(8,128)(2,1)S(1)}, bf16[256,4096]{1,0:T(8,128)(2,1)}, u32[]{:S(2)}) copy-start(bf16[256,4096]{1,0:T(8,128)(2,1)} %param.18) | copy-start | bytes 6291460
Sparse Core Ops, SparseCore 0:
  12.4 63.8 all-gather.1
  786.4 33.0 reduce-scatter.1
